TPU v7x, 32 devices: a whole 2x2x4 slice. The times are simulated.
32 devices in a mesh: sp: 8 (over z, y), tp: 4 (over x, core).
Axes of the slice: x: 2, y: 2, z: 4, core: 2. Of those that a mesh axis runs over, the one named last changes fastest.
Arguments:
- tokens: bfloat16 [1024, 2048], P(('sp', 'tp')), may hold values from -64 to 64, as said below
- query_one: bfloat16 [2048, 256], P(None, 'tp'), may hold values from -0.125 to 0.125
- query_two: bfloat16 [2048, 256], P(None, 'tp'), may hold values from -0.125 to 0.125
- key_one: bfloat16 [2048, 256], P(None, 'tp'), may hold values from -0.125 to 0.125
- key_two: bfloat16 [2048, 256], P(None, 'tp'), may hold values from -0.125 to 0.125
- value_weight: bfloat16 [2048, 512], P(None, 'tp'), may hold values from -0.125 to 0.125
- mixing: float32 [4], P('tp'), may hold values from 0.3 to 0.8
- out_weight: bfloat16 [512, 2048], replicated, may hold values from -0.25 to 0.25
- head_gain: float32 [128], replicated, may hold values from 0.1 to 1.9
Outputs:
- attended: bfloat16 [1024, 2048], P(('sp', 'tp'))
Inputs may be any that keep to these rules, and one draw needn't show every extreme that they name: `tokens`: Real-valued activations.
All inputs are finite; a program needn't handle non-finite values.
Results may differ from a plain program's by a relative error of at most 0.012.
The roundings to bfloat16 on the way count: a program that leaves them out, or rounds other values in their place, can miss the bound.
Values may be sent and summed in bfloat16 or wider, within the bound.
No kernel may reach another device: no remote copies, remote signals or barrier semaphores. Data moves between devices by JAX's collectives and lax.ppermute only.
A program may use at most 64 MiB of HBM per device.

v0:
```python
import math
import jax
import jax.numpy as jnp
from jax import lax
from jax.sharding import PartitionSpec as P

HEAD = 64
GRID_W = 64
epsilon = 1e-06
theta_base = 10000.0
floor_value = -1e30


def grid_turn(field, positions):
    quarter = field.shape[-1] // 4
    half = 2 * quarter
    freqs = theta_base ** (-jnp.arange(quarter, dtype=jnp.float32) / quarter)
    row_angle = (positions // GRID_W).astype(jnp.float32)[:, None] * freqs
    col_angle = (positions % GRID_W).astype(jnp.float32)[:, None] * freqs

    def turn(segment, angle):
        cosine = jnp.cos(angle)[:, None, :]
        sine = jnp.sin(angle)[:, None, :]
        first = segment[..., :quarter]
        second = segment[..., quarter:]
        return jnp.concatenate(
            [first * cosine - second * sine, first * sine + second * cosine], axis=-1
        )

    return jnp.concatenate(
        [turn(field[..., :half], row_angle), turn(field[..., half:], col_angle)], axis=-1
    )


def one_map(state, queries, keys, values):
    peak, total, summed = state
    scores = jnp.einsum(
        "qhd,khd->qhk", queries, keys, preferred_element_type=jnp.float32
    ) * HEAD ** (-0.5)
    new_peak = jnp.maximum(peak, jnp.max(scores, axis=-1))
    factor = jnp.exp(peak - new_peak)
    weights = jnp.exp(scores - new_peak[..., None])
    total = total * factor + jnp.sum(weights, axis=-1)
    summed = summed * factor[..., None] + jnp.einsum(
        "qhk,khe->qhe", weights.astype(jnp.bfloat16), values, preferred_element_type=jnp.float32
    )
    return (new_peak, total, summed)


def make_absorb(q_first, q_second, head_local):
    cols = head_local * HEAD

    def absorb(carry, piece, start):
        count = piece.shape[0]
        width = math.gcd(count, 2048)

        def step(index, state):
            block = lax.dynamic_slice_in_dim(piece, index * width, width, 0)
            keys_first = block[:, :cols].reshape(width, head_local, HEAD)
            keys_second = block[:, cols : 2 * cols].reshape(width, head_local, HEAD)
            values = block[:, 2 * cols :].reshape(width, head_local, 2 * HEAD)
            return (
                one_map(state[0], q_first, keys_first, values),
                one_map(state[1], q_second, keys_second, values),
            )

        return lax.fori_loop(0, count // width, step, carry)

    return absorb


def per_device(
    tokens, query_one, query_two, key_one, key_two, value_weight, mixing, out_weight, head_gain
):
    groups = lax.axis_size("tp")
    own_rows = tokens.shape[0]
    row_count = own_rows * groups
    head_cols = query_one.shape[1]
    head_local = head_cols // HEAD
    joined = jnp.concatenate([query_one, query_two, key_one, key_two, value_weight], axis=1)
    projected = jnp.dot(
        lax.all_gather(tokens, "tp", axis=0, tiled=True), joined, preferred_element_type=jnp.float32
    )
    positions = lax.axis_index("sp") * row_count + jnp.arange(row_count, dtype=jnp.int32)

    def heads_of(lower, upper):
        return projected[:, lower:upper].reshape(row_count, head_local, HEAD)

    q_first = grid_turn(heads_of(0, head_cols), positions).astype(jnp.bfloat16)
    q_second = grid_turn(heads_of(head_cols, 2 * head_cols), positions).astype(jnp.bfloat16)
    k_first = grid_turn(heads_of(2 * head_cols, 3 * head_cols), positions).astype(jnp.bfloat16)
    k_second = grid_turn(heads_of(3 * head_cols, 4 * head_cols), positions).astype(jnp.bfloat16)
    values = projected[:, 4 * head_cols :].astype(jnp.bfloat16)
    packed = jnp.concatenate(
        [k_first.reshape(row_count, head_cols), k_second.reshape(row_count, head_cols), values],
        axis=1,
    )
    absorb = make_absorb(q_first, q_second, head_local)
    empty = (
        jnp.full((row_count, head_local), floor_value, jnp.float32),
        jnp.zeros((row_count, head_local), jnp.float32),
        jnp.zeros((row_count, head_local, 2 * HEAD), jnp.float32),
    )
    gathered = lax.all_gather(packed, "sp", axis=0, tiled=True)
    first_map, second_map = absorb((empty, empty), gathered, 0)
    mixed = first_map[2] / first_map[1][..., None] - mixing[None, :, None] * (
        second_map[2] / second_map[1][..., None]
    )
    normed = (
        mixed * lax.rsqrt(jnp.mean(mixed * mixed, axis=-1, keepdims=True) + epsilon) * head_gain
    )
    heads = normed.astype(jnp.bfloat16).reshape(row_count, head_local * 2 * HEAD)
    regrouped = lax.all_to_all(heads, "tp", split_axis=0, concat_axis=1, tiled=True)
    summed = jnp.dot(regrouped, out_weight, preferred_element_type=jnp.float32)
    return summed.astype(jnp.bfloat16)


def solution(mesh):
    in_specs = (
        P(("sp", "tp"), None),
        P(None, "tp"),
        P(None, "tp"),
        P(None, "tp"),
        P(None, "tp"),
        P(None, "tp"),
        P("tp"),
        P(),
        P(),
    )
    out_specs = P(("sp", "tp"), None)
    return jax.shard_map(
        per_device, mesh=mesh, in_specs=in_specs, out_specs=out_specs, check_vma=False
    )
```

profile of v0, /device:TPU:0, one launch (start us, length us, event | category | flops | bytes accessed | tf_op | source)
XLA Modules:
  0.0 59.8 jit_solution(14919113349166023938)
XLA Ops:
  0.0 0.0 copy-start
  0.0 0.0 copy-start.1
  0.0 0.0 copy-start.2
  0.0 1.4 %copy.19 = bf16[2048,64]{1,0:T(8,128)(2,1)S(1)} copy(bf16[2048,64]{0,1:T(8,128)(2,1)} %param.10) | data formatting | bytes 524288 | tf_op args[1]
  1.4 2.0 %copy.20 = bf16[2048,64]{1,0:T(8,128)(2,1)} copy(bf16[2048,64]{0,1:T(8,128)(2,1)} %param.11) | data formatting | bytes 524288 | tf_op args[2]
  3.4 2.0 %copy.21 = bf16[2048,64]{1,0:T(8,128)(2,1)} copy(bf16[2048,64]{0,1:T(8,128)(2,1)} %param.12) | data formatting | bytes 524288 | tf_op args[3]
  5.3 0.0 copy-done.1
  5.3 1.0 %copy.22 = bf16[2048,64]{1,0:T(8,128)(2,1)} copy(bf16[2048,64]{0,1:T(8,128)(2,1)S(1)} %copy-done.1) | data formatting | bytes 524288 | tf_op args[4]
  6.4 0.0 copy-done.2
  6.4 8.6 %all_gather.6 = bf16[128,2048]{1,0:T(8,128)(2,1)S(1)} all-gather(bf16[32,2048]{1,0:T(8,128)(2,1)S(1)} %copy-done.2), channel_id=1, replica_groups=mesh['sp'=8,'tp'=4] {'tp'}, dimensions={0}, use_global_device_ids=true | all-gather | bytes 655360 | tf_op jit(solution)/shard_map/all_gather | solution.py:82
  15.0 4.1 %concatenate.63 = bf16[2048,384]{1,0:T(8,128)(2,1)} concatenate(bf16[2048,64]{1,0:T(8,128)(2,1)S(1)} %copy.19, bf16[2048,64]{1,0:T(8,128)(2,1)} %copy.20, bf16[2048,64]{1,0:T(8,128)(2,1)} %copy.21, bf16[2048,64]{1,0:T(8,128)(2,1)} %copy.22, bf16[2048,128]{1,0:T(8,128)(2,1)} %param.14), dimensions={1} | concatenate | bytes 3145728 | tf_op jit(solution)/shard_map/concatenate | solution.py:80
  19.1 2.0 %convolution_bitcast_fusion = f32[128,384]{0,1:T(8,128)S(1)} fusion(bf16[2048,384]{1,0:T(8,128)(2,1)} %concatenate.63, bf16[128,2048]{1,0:T(8,128)(2,1)S(1)} %all_gather.6), kind=kOutput, calls=%fused_computation.3 | convolution fusion | flops 201326592 | bytes 2293760 | tf_op jit(solution)/shard_map/dot_general | solution.py:81
  21.2 0.1 constant_dynamic-update-slice_fusion.7
  21.3 0.1 constant_dynamic-update-slice_fusion.6
  21.4 0.1 constant_dynamic-update-slice_fusion.5
  21.5 0.1 constant_dynamic-update-slice_fusion.4
  21.7 0.1 constant_dynamic-update-slice_fusion.3
  21.8 0.1 constant_dynamic-update-slice_fusion.2
  21.9 0.1 constant_dynamic-update-slice_fusion.1
  22.1 0.1 constant_dynamic-update-slice_fusion
  22.2 27.5 %all_gather.7 = bf16[1024,256]{0,1:T(8,128)(2,1)S(1)} all-gather(bf16[128,256]{0,1:T(8,128)(2,1)S(1)} %fusion.22), channel_id=1, replica_groups=mesh['sp'=8,'tp'=4] {'sp'}, dimensions={0}, use_global_device_ids=true | all-gather | bytes 589824 | tf_op jit(solution)/shard_map/all_gather | solution.py:104
  49.7 0.2 fusion.108
  49.8 0.0 copy-start.3
  49.8 0.3 fusion.117
  50.2 0.2 fusion.10
  51.0 0.3 fusion.118
  51.4 0.2 fusion.8
  51.5 0.3 fusion.5
  51.8 0.4 multiply_reduce_fusion
  52.2 0.0 copy-done.3
  52.2 0.1 multiply_convert_fusion
  52.3 6.3 %all_to_all.19 = bf16[4,32,128]{2,1,0:T(8,128)(2,1)S(1)} all-to-all(bf16[4,32,128]{2,1,0:T(8,128)(2,1)S(1)} %bitcast.110), channel_id=1, replica_groups=mesh['sp'=8,'tp'=4] {'tp'}, dimensions={0} | all-to-all | bytes 65536 | tf_op jit(solution)/shard_map/all_to_all | solution.py:113
  58.6 0.0 copy-done
  58.6 1.1 %convolution_convert_fusion = bf16[32,2048]{1,0:T(8,128)(2,1)} fusion(bf16[512,2048]{1,0:T(8,128)(2,1)S(1)} %copy-done, bf16[4,32,128]{2,1,0:T(8,128)(2,1)S(1)} %all_to_all.19), kind=kOutput, calls=%fused_computation | convolution fusion | flops 67174400 | bytes 2260992 | tf_op jit(solution)/shard_map/dot_general | solution.py:114
  (9 shorter events, 0.1 us)
Async XLA Ops:
  0.0 58.6 %copy-start = (bf16[512,2048]{1,0:T(8,128)(2,1)S(1)}, bf16[512,2048]{1,0:T(8,128)(2,1)}, u32[]{:S(2)}) copy-start(bf16[512,2048]{1,0:T(8,128)(2,1)} %param.16) | copy-start | bytes 6291460
  0.0 5.3 %copy-start.1 = (bf16[2048,64]{0,1:T(8,128)(2,1)S(1)}, bf16[2048,64]{0,1:T(8,128)(2,1)}, u32[]{:S(2)}) copy-start(bf16[2048,64]{0,1:T(8,128)(2,1)} %param.13) | copy-start | bytes 786436
  0.0 6.4 %copy-start.2 = (bf16[32,2048]{1,0:T(8,128)(2,1)S(1)}, bf16[32,2048]{1,0:T(8,128)(2,1)}, u32[]{:S(2)}) copy-start(bf16[32,2048]{1,0:T(8,128)(2,1)} %param.9) | copy-start | bytes 393220
  49.8 2.4 %copy-start.3 = (f32[128]{0:T(128)S(1)}, f32[128]{0:T(128)}, u32[]{:S(2)}) copy-start(f32[128]{0:T(128)} %param.17) | copy-start | bytes 1540
where the time goes:
time: 60.1 us; the launch traced here: 59.8 us
  blocking collectives  42.4 us (71%)
  local copies, waits for them, and re-layouts  10.5 us (17%)
  matrix products  4.48 us (7%)
  other arithmetic  1.64 us (3%)
  between operations  0.75 us (1%)
    all_gather x1, blocking collectives, per_device(): gathered = lax.all_gather(packed, 'sp', axis=0, tiled=True)  27.5 us
    all_gather x1, blocking collectives, per_device(): lax.all_gather(tokens, 'tp', axis=0, tiled=True)  8.64 us
    unnamed x12, local copies, waits for them, and re-layouts  6.35 us
    all_to_all x1, blocking collectives, per_device(): lax.all_to_all(heads, 'tp', split_axis=0, concat_axis=1, tiled=True)  6.3 us
    concatenate x1, local copies, waits for them, and re-layouts, per_device(): jnp.concatenate([query_one, query_two, key_one, key_two, value_weight], a...  4.1 us
    dot_general x1, matrix products, per_device(): jnp.dot(lax.all_gather(tokens, 'tp', axis=0, tiled=True), joined, preferr...  2.01 us

commit v1 on v0

--- a/solution.py
+++ b/solution.py
@@ -110,7 +110,9 @@
         mixed * lax.rsqrt(jnp.mean(mixed * mixed, axis=-1, keepdims=True) + epsilon) * head_gain
     )
     heads = normed.astype(jnp.bfloat16).reshape(row_count, head_local * 2 * HEAD)
-    regrouped = lax.all_to_all(heads, "tp", split_axis=0, concat_axis=1, tiled=True)
+    pieces = jnp.split(heads, lax.axis_size("tp"), axis=0)
+    incoming = lax.all_to_all(jnp.stack(pieces), "tp", 0, 0)
+    regrouped = jnp.concatenate(incoming, axis=1)
     summed = jnp.dot(regrouped, out_weight, preferred_element_type=jnp.float32)
     return summed.astype(jnp.bfloat16)
 

time: 60.1 us -> 60.1 us (level)
  no operation moved by 1% of the time
where the time goes in v1:
time: 60.1 us; the launch traced here: 59.8 us
  blocking collectives  42.4 us (71%)
  local copies, waits for them, and re-layouts  10.5 us (17%)
  matrix products  4.48 us (7%)
  other arithmetic  1.65 us (3%)
  between operations  0.76 us (1%)
    all_gather x1, blocking collectives, per_device(): gathered = lax.all_gather(packed, 'sp', axis=0, tiled=True)  27.5 us
    all_gather x1, blocking collectives, per_device(): lax.all_gather(tokens, 'tp', axis=0, tiled=True)  8.64 us
    unnamed x12, local copies, waits for them, and re-layouts  6.35 us
    all_to_all x1, blocking collectives, per_device(): incoming = lax.all_to_all(jnp.stack(pieces), 'tp', 0, 0)  6.3 us
    concatenate x1, local copies, waits for them, and re-layouts, per_device(): jnp.concatenate([query_one, query_two, key_one, key_two, value_weight], a...  4.1 us
    dot_general x1, matrix products, per_device(): jnp.dot(lax.all_gather(tokens, 'tp', axis=0, tiled=True), joined, preferr...  2.01 us

profile of v1, /device:TPU:0, one launch (start us, length us, event | category | flops | bytes accessed | tf_op | source)
XLA Modules:
  0.0 59.8 jit_solution(15953610616703112047)
XLA Ops:
  0.0 0.0 copy-start
  0.0 0.0 copy-start.1
  0.0 0.0 copy-start.2
  0.0 1.4 %copy.14 = bf16[2048,64]{1,0:T(8,128)(2,1)S(1)} copy(bf16[2048,64]{0,1:T(8,128)(2,1)} %param.10) | data formatting | bytes 524288 | tf_op args[1]
  1.4 2.0 %copy.15 = bf16[2048,64]{1,0:T(8,128)(2,1)} copy(bf16[2048,64]{0,1:T(8,128)(2,1)} %param.11) | data formatting | bytes 524288 | tf_op args[2]
  3.4 2.0 %copy.16 = bf16[2048,64]{1,0:T(8,128)(2,1)} copy(bf16[2048,64]{0,1:T(8,128)(2,1)} %param.12) | data formatting | bytes 524288 | tf_op args[3]
  5.3 0.0 copy-done.1
  5.3 1.0 %copy.17 = bf16[2048,64]{1,0:T(8,128)(2,1)} copy(bf16[2048,64]{0,1:T(8,128)(2,1)S(1)} %copy-done.1) | data formatting | bytes 524288 | tf_op args[4]
  6.4 0.0 copy-done.2
  6.4 8.6 %all_gather.6 = bf16[128,2048]{1,0:T(8,128)(2,1)S(1)} all-gather(bf16[32,2048]{1,0:T(8,128)(2,1)S(1)} %copy-done.2), channel_id=1, replica_groups=mesh['sp'=8,'tp'=4] {'tp'}, dimensions={0}, use_global_device_ids=true | all-gather | bytes 655360 | tf_op jit(solution)/shard_map/all_gather | solution.py:82
  15.0 4.1 %concatenate.63 = bf16[2048,384]{1,0:T(8,128)(2,1)} concatenate(bf16[2048,64]{1,0:T(8,128)(2,1)S(1)} %copy.14, bf16[2048,64]{1,0:T(8,128)(2,1)} %copy.15, bf16[2048,64]{1,0:T(8,128)(2,1)} %copy.16, bf16[2048,64]{1,0:T(8,128)(2,1)} %copy.17, bf16[2048,128]{1,0:T(8,128)(2,1)} %param.14), dimensions={1} | concatenate | bytes 3145728 | tf_op jit(solution)/shard_map/concatenate | solution.py:80
  19.1 2.0 %convolution_bitcast_fusion = f32[128,384]{0,1:T(8,128)S(1)} fusion(bf16[2048,384]{1,0:T(8,128)(2,1)} %concatenate.63, bf16[128,2048]{1,0:T(8,128)(2,1)S(1)} %all_gather.6), kind=kOutput, calls=%fused_computation.3 | convolution fusion | flops 201326592 | bytes 2293760 | tf_op jit(solution)/shard_map/dot_general | solution.py:81
  21.2 0.1 constant_dynamic-update-slice_fusion.7
  21.3 0.1 constant_dynamic-update-slice_fusion.6
  21.4 0.1 constant_dynamic-update-slice_fusion.5
  21.5 0.1 constant_dynamic-update-slice_fusion.4
  21.7 0.1 constant_dynamic-update-slice_fusion.3
  21.8 0.1 constant_dynamic-update-slice_fusion.2
  21.9 0.1 constant_dynamic-update-slice_fusion.1
  22.1 0.1 constant_dynamic-update-slice_fusion
  22.2 27.5 %all_gather.7 = bf16[1024,256]{0,1:T(8,128)(2,1)S(1)} all-gather(bf16[128,256]{0,1:T(8,128)(2,1)S(1)} %fusion.23), channel_id=1, replica_groups=mesh['sp'=8,'tp'=4] {'sp'}, dimensions={0}, use_global_device_ids=true | all-gather | bytes 589824 | tf_op jit(solution)/shard_map/all_gather | solution.py:104
  49.7 0.2 fusion.109
  49.8 0.0 copy-start.3
  49.8 0.3 fusion.118
  50.2 0.2 fusion.10
  51.0 0.3 fusion.119
  51.4 0.2 fusion.8
  51.5 0.3 fusion.5
  51.8 0.4 multiply_reduce_fusion
  52.2 0.0 copy-done.3
  52.2 0.1 fusion.22
  52.3 6.3 %all_to_all.5 = bf16[4,32,128]{2,1,0:T(8,128)(2,1)S(1)} all-to-all(bf16[4,32,128]{2,1,0:T(8,128)(2,1)S(1)} %pad_maximum_fusion), channel_id=1, replica_groups=mesh['sp'=8,'tp'=4] {'tp'}, dimensions={0} | all-to-all | bytes 65536 | tf_op jit(solution)/shard_map/all_to_all | solution.py:114
  58.6 0.0 copy-done
  58.6 1.1 %convolution_convert_fusion = bf16[32,2048]{1,0:T(8,128)(2,1)} fusion(bf16[512,2048]{1,0:T(8,128)(2,1)S(1)} %copy-done, bf16[4,32,128]{2,1,0:T(8,128)(2,1)S(1)} %all_to_all.5), kind=kOutput, calls=%fused_computation | convolution fusion | flops 67174400 | bytes 2260992 | tf_op jit(solution)/shard_map/dot_general | solution.py:116
  (11 shorter events, 0.1 us)
Async XLA Ops:
  0.0 58.6 %copy-start = (bf16[512,2048]{1,0:T(8,128)(2,1)S(1)}, bf16[512,2048]{1,0:T(8,128)(2,1)}, u32[]{:S(2)}) copy-start(bf16[512,2048]{1,0:T(8,128)(2,1)} %param.16) | copy-start | bytes 6291460
  0.0 5.3 %copy-start.1 = (bf16[2048,64]{0,1:T(8,128)(2,1)S(1)}, bf16[2048,64]{0,1:T(8,128)(2,1)}, u32[]{:S(2)}) copy-start(bf16[2048,64]{0,1:T(8,128)(2,1)} %param.13) | copy-start | bytes 786436
  0.0 6.4 %copy-start.2 = (bf16[32,2048]{1,0:T(8,128)(2,1)S(1)}, bf16[32,2048]{1,0:T(8,128)(2,1)}, u32[]{:S(2)}) copy-start(bf16[32,2048]{1,0:T(8,128)(2,1)} %param.9) | copy-start | bytes 393220
  49.8 2.4 %copy-start.3 = (f32[128]{0:T(128)S(1)}, f32[128]{0:T(128)}, u32[]{:S(2)}) copy-start(f32[128]{0:T(128)} %param.17) | copy-start | bytes 1540
